TPU v7x, 32 devices: a whole 2x2x4 slice. The times are simulated.
32 devices in a mesh: fs: 4 (over z), rep: 2 (over y), tp: 4 (over x, core).
Axes of the slice: x: 2, y: 2, z: 4, core: 2. Of those that a mesh axis runs over, the one named last changes fastest.
Arguments:
- saved_input: bfloat16 [5120, 3072], P(('fs', 'rep')), may hold values from -6 to 6
- key_cotangent: bfloat16 [5120, 1024], P(('fs', 'rep'), 'tp'), may hold values from -0.0625 to 0.0625
- value_cotangent: bfloat16 [5120, 2048], P(('fs', 'rep'), 'tp'), may hold values from -0.0625 to 0.0625
- key_factor: bfloat16 [3072, 256], replicated, may hold values from -0.375 to 0.375
- value_factor: bfloat16 [3072, 256], replicated, may hold values from -0.375 to 0.375
- key_weight: float32 [3072, 1024], P(('fs', 'rep'), 'tp'), may hold values from -0.109375 to 0.109375
- value_weight: float32 [3072, 2048], P(('fs', 'rep'), 'tp'), may hold values from -0.109375 to 0.109375
- key_first: float32 [256, 1024], P(None, 'tp'), as said below
- key_second: float32 [256, 1024], P(None, 'tp'), may hold values from 0.05 to 1
- value_first: float32 [256, 2048], P(None, 'tp'), as said below
- value_second: float32 [256, 2048], P(None, 'tp'), may hold values from 0.05 to 1
Outputs:
- key_weight_new: float32 [3072, 1024], P(('fs', 'rep'), 'tp')
- value_weight_new: float32 [3072, 2048], P(('fs', 'rep'), 'tp')
- key_first_new: float32 [256, 1024], P(None, 'tp')
- key_second_new: float32 [256, 1024], P(None, 'tp')
- value_first_new: float32 [256, 2048], P(None, 'tp')
- value_second_new: float32 [256, 2048], P(None, 'tp')
- key_step: float32 [3072, 1024], P(('fs', 'rep'), 'tp')
- value_step: float32 [3072, 2048], P(('fs', 'rep'), 'tp')
- key_copy: bfloat16 [3072, 1024], P(None, 'tp')
- value_copy: bfloat16 [3072, 2048], P(None, 'tp')
Inputs may be any that keep to these rules, and one draw needn't show every extreme that they name: `key_first`: real-valued moments whose scale differs from head to head. `value_first`: real-valued moments whose scale differs from head to head.
All inputs are finite; a program needn't handle non-finite values.
Results may differ from a plain program's by a relative error of at most 0.004.
Values may be sent and summed in bfloat16 or wider, within the bound.
No kernel may reach another device: no remote copies, remote signals or barrier semaphores. Data moves between devices by JAX's collectives and lax.ppermute only.
A program may use at most 64 MiB of HBM per device.

v0:
```python
import jax
import jax.numpy as jnp
from jax import lax
from jax.sharding import PartitionSpec as P

DK = 1024
DV = 2048
RK = 256
RV = 256
first_decay = 0.8
second_decay = 0.9
epsilon = 1e-08
learn_rate = 0.01


def split_contract(basis, cotangent):
    upper = basis.astype(jnp.bfloat16)
    lower = (basis - upper.astype(jnp.float32)).astype(jnp.bfloat16)
    dims = (((0,), (0,)), ((), ()))
    high_part = lax.dot_general(upper, cotangent, dims, preferred_element_type=jnp.float32)
    low_part = lax.dot_general(lower, cotangent, dims, preferred_element_type=jnp.float32)
    return high_part + low_part


def moments(projection, first, second):
    first_new = first_decay * first + (1.0 - first_decay) * projection
    second_new = second_decay * second + (1.0 - second_decay) * projection * projection
    normed = first_new / (jnp.sqrt(second_new) + epsilon)
    return (first_new, second_new, normed)


def body(
    saved_input,
    key_cotangent,
    value_cotangent,
    key_factor,
    value_factor,
    key_weight,
    value_weight,
    key_first,
    key_second,
    value_first,
    value_second,
):
    local_rows = key_weight.shape[0]
    row_offset = lax.axis_index(("fs", "rep")) * local_rows
    key_rows = lax.dynamic_slice_in_dim(key_factor, row_offset, local_rows, 0).astype(jnp.float32)
    value_rows = lax.dynamic_slice_in_dim(value_factor, row_offset, local_rows, 0).astype(
        jnp.float32
    )
    key_basis = jnp.dot(saved_input, key_factor, preferred_element_type=jnp.float32)
    key_part = split_contract(key_basis, key_cotangent)
    value_basis = jnp.dot(saved_input, value_factor, preferred_element_type=jnp.float32)
    value_part = split_contract(value_basis, value_cotangent)
    key_projected, value_projected = lax.psum((key_part, value_part), ("fs", "rep"))
    key_first_new, key_second_new, key_normed = moments(key_projected, key_first, key_second)
    value_first_new, value_second_new, value_normed = moments(
        value_projected, value_first, value_second
    )
    local_squares = jnp.sum(key_normed * key_normed) + jnp.sum(value_normed * value_normed)
    squares = lax.psum(local_squares, "tp")
    entries = jnp.float32(RK * DK + RV * DV)
    shrink = jnp.sqrt(entries / (entries + squares))
    key_step = shrink * jnp.dot(key_rows, key_normed, precision=lax.Precision.HIGHEST)
    value_step = shrink * jnp.dot(value_rows, value_normed, precision=lax.Precision.HIGHEST)
    key_weight_new = key_weight - learn_rate * key_step
    value_weight_new = value_weight - learn_rate * value_step
    key_copy, value_copy = (
        lax.all_gather(key_weight_new.astype(jnp.bfloat16), ("fs", "rep"), axis=0, tiled=True),
        lax.all_gather(value_weight_new.astype(jnp.bfloat16), ("fs", "rep"), axis=0, tiled=True),
    )
    return (
        key_weight_new,
        value_weight_new,
        key_first_new,
        key_second_new,
        value_first_new,
        value_second_new,
        key_step,
        value_step,
        key_copy,
        value_copy,
    )


def solution(mesh):
    in_specs = (
        P(("fs", "rep"), None),
        P(("fs", "rep"), "tp"),
        P(("fs", "rep"), "tp"),
        P(),
        P(),
        P(("fs", "rep"), "tp"),
        P(("fs", "rep"), "tp"),
        P(None, "tp"),
        P(None, "tp"),
        P(None, "tp"),
        P(None, "tp"),
    )
    out_specs = (
        P(("fs", "rep"), "tp"),
        P(("fs", "rep"), "tp"),
        P(None, "tp"),
        P(None, "tp"),
        P(None, "tp"),
        P(None, "tp"),
        P(("fs", "rep"), "tp"),
        P(("fs", "rep"), "tp"),
        P(None, "tp"),
        P(None, "tp"),
    )
    return jax.shard_map(body, mesh=mesh, in_specs=in_specs, out_specs=out_specs, check_vma=False)
```

profile of v0, /device:TPU:0, one launch (start us, length us, event | category | flops | bytes accessed | tf_op | source)
XLA Modules:
  0.0 225.4 jit_solution(12211310105299718607)
XLA Ops:
  7.2 0.0 copy-start
  7.2 0.0 copy-start.2
  7.2 0.0 all-reduce.3.cloned.1.call-start
  7.2 1.3 copy-done
  8.6 0.0 copy-start.12
  8.6 3.4 %fusion.17 = f32[640,256]{1,0:T(8,128)S(1)} fusion(bf16[640,3072]{1,0:T(8,128)(2,1)} %param.11, bf16[3072,256]{1,0:T(8,128)(2,1)S(1)} %copy-done), kind=kOutput, calls=%fused_computation.31 | convolution fusion | flops 1006632960 | bytes 6160384 | tf_op jit(solution)/shard_map/dot_general | solution.py:53
  12.0 0.0 copy-done.2
  12.1 0.4 fusion.5
  12.5 0.0 copy-start.11
  12.5 1.2 convolution_add_fusion
  13.7 0.0 copy-done.12
  13.7 0.3 copy-done.11
  13.9 0.0 copy-start.5
  13.9 1.2 fusion.16
  15.1 0.0 copy-done.5
  15.1 0.0 copy-start.8
  15.2 0.3 fusion.8
  15.5 1.0 convolution_add_fusion.1
  16.5 0.0 all-reduce.3.cloned.1.call-update
  16.5 0.0 all-gather.3.cloned.1.call-start
  16.6 77.9 %all-reduce.3.cloned.1.call-done = (f32[256,256]{1,0:T(8,128)}, f32[256,512]{1,0:T(8,128)}) async-done(((f32[256,256]{1,0:T(8,128)}, f32[256,512]{1,0:T(8,128)}), (f32[256,256]{1,0:T(8,128)}, f32[256,512]{1,0:T(8,128)})) %all-reduce.3.cloned.1.call-update) | async-done | bytes 786448 | tf_op jit(solution)/shard_map/psum | solution.py:55
  94.5 0.0 copy-start.10
  94.5 0.0 copy-done.8
  94.5 0.0 copy-start.9
  94.5 2.2 multiply_reduce_fusion
  96.7 0.0 copy-start.3
  96.7 0.0 copy-start.4
  96.7 0.0 copy-done.10
  96.7 2.2 multiply_reduce_fusion.1
  98.9 0.0 copy-start.6
  98.9 0.0 copy-start.7
  100.2 6.2 %psum.23 = f32[]{:T(128)} all-reduce(f32[]{:T(128)S(6)} %add.59), channel_id=1, replica_groups=mesh['fs'=4,'rep'=2,'tp'=4] {'tp'}, use_global_device_ids=true, to_apply=%region_4.0 | all-reduce | flops 1 | bytes 8 | tf_op jit(solution)/shard_map/psum | solution.py:61
  107.1 0.0 copy-done.9
  107.1 2.3 %fusion.13 = (bf16[384,256]{1,0:T(8,128)(2,1)}, f32[384,256]{1,0:T(8,128)}, f32[384,256]{1,0:T(8,128)}) fusion(f32[384,256]{1,0:T(8,128)S(1)} %copy-done.9, f32[256,256]{1,0:T(8,128)S(1)} %get-tuple-element.36, f32[256,256]{1,0:T(8,128)S(1)} %get-tuple-element.37, bf16[3072,256]{1,0:T(8,128)(2,1)} %param.14, s32[]{:T(128)S(6)} %select_n.4, f32[]{:T(128)S(6)} %sqrt.11), kind=kOutput, calls=%fused_computation.29 | convolution fusion | flops 302514176 | bytes 2097160 | tf_op jit(solution)/shard_map/dot_general | solution.py:64
  109.4 0.0 all-gather.3.cloned.1.call-update
  109.5 0.0 all-gather.5.cloned.1.call-start
  109.5 0.0 copy-done.3
  109.5 0.0 copy-done.4
  109.5 3.2 %fusion.12 = (bf16[384,512]{1,0:T(8,128)(2,1)}, f32[384,512]{1,0:T(8,128)}, f32[384,512]{1,0:T(8,128)}) fusion(f32[384,512]{1,0:T(8,128)} %param.17, f32[256,512]{1,0:T(8,128)S(1)} %get-tuple-element.38, f32[256,512]{1,0:T(8,128)S(1)} %get-tuple-element.39, bf16[3072,256]{1,0:T(8,128)(2,1)S(1)} %copy-done, s32[]{:T(128)S(6)} %select_n.4, f32[]{:T(128)S(6)} %sqrt.11), kind=kOutput, calls=%fused_computation.28 | convolution fusion | flops 605028352 | bytes 3997704 | tf_op jit(solution)/shard_map/dot_general | solution.py:65
  112.7 0.0 copy-done.6
  112.7 0.0 copy-done.7
  112.7 0.0 all-gather.5.cloned.1.call-update
  112.7 40.5 %all-gather.3.cloned.1.call-done = bf16[3072,256]{1,0:T(8,128)(2,1)} async-done(((bf16[384,256]{1,0:T(8,128)(2,1)}), bf16[3072,256]{1,0:T(8,128)(2,1)}) %all-gather.3.cloned.1.call-update) | async-done | bytes 1572880 | tf_op jit(solution)/shard_map/all_gather | solution.py:69
  153.2 61.2 %all-gather.5.cloned.1.call-done = bf16[3072,512]{1,0:T(8,128)(2,1)} async-done(((bf16[384,512]{1,0:T(8,128)(2,1)}), bf16[3072,512]{1,0:T(8,128)(2,1)}) %all-gather.5.cloned.1.call-update) | async-done | bytes 3145744 | tf_op jit(solution)/shard_map/all_gather | solution.py:70
  214.4 0.0 copy-start.1
  214.4 2.8 %copy.25 = bf16[3072,256]{1,0:T(8,128)(2,1)} copy(bf16[3072,256]{1,0:T(8,128)(2,1)} %all-gather.3.cloned.1.call-done) | data formatting | bytes 3145728
  217.2 0.0 copy-done.1
  217.2 1.7 copy.26
Async XLA Ops:
  7.2 1.4 copy-start
  7.2 4.9 %copy-start.2 = (bf16[640,512]{1,0:T(8,128)(2,1)S(1)}, bf16[640,512]{1,0:T(8,128)(2,1)}, u32[]{:S(2)}) copy-start(bf16[640,512]{1,0:T(8,128)(2,1)} %param.13) | copy-start | bytes 1966084
  7.2 87.3 %all-reduce.3.cloned.1.call-start = ((), (), s32[]{:S(2)}) async-start(), calls=%async_computation.2 | async-start | bytes 1572864 | tf_op jit(solution)/shard_map/psum | solution.py:55
  8.6 5.1 %copy-start.12 = (bf16[640,3072]{1,0:T(8,128)(2,1)S(1)}, bf16[640,3072]{1,0:T(8,128)(2,1)}, u32[]{:S(2)}) copy-start(bf16[640,3072]{1,0:T(8,128)(2,1)} %param.11) | copy-start | bytes 11796484
  12.5 1.5 copy-start.11
  13.9 1.2 copy-start.5
  15.1 79.4 %copy-start.8 = (f32[256,512]{1,0:T(8,128)S(1)}, f32[256,512]{1,0:T(8,128)}, u32[]{:S(2)}) copy-start(f32[256,512]{1,0:T(8,128)} %param.21) | copy-start | bytes 1572868
  16.5 136.7 %all-gather.3.cloned.1.call-start = ((), (), s32[]{:S(2)}) async-start(), calls=%async_computation | async-start | bytes 1769472 | tf_op jit(solution)/shard_map/all_gather | solution.py:69
  94.5 2.2 copy-start.10
  94.5 12.6 %copy-start.9 = (f32[384,256]{1,0:T(8,128)S(1)}, f32[384,256]{1,0:T(8,128)}, u32[]{:S(2)}) copy-start(f32[384,256]{1,0:T(8,128)} %param.16) | copy-start | bytes 1179652
  96.7 12.8 %copy-start.3 = (f32[256,512]{1,0:T(8,128)}, f32[256,512]{1,0:T(8,128)S(1)}, u32[]{:S(2)}) copy-start(f32[256,512]{1,0:T(8,128)S(1)} %get-tuple-element.39) | copy-start | bytes 1572868
  96.7 12.8 %copy-start.4 = (f32[256,512]{1,0:T(8,128)}, f32[256,512]{1,0:T(8,128)S(1)}, u32[]{:S(2)}) copy-start(f32[256,512]{1,0:T(8,128)S(1)} %get-tuple-element.38) | copy-start | bytes 1572868
  98.9 13.8 %copy-start.6 = (f32[256,256]{1,0:T(8,128)}, f32[256,256]{1,0:T(8,128)S(1)}, u32[]{:S(2)}) copy-start(f32[256,256]{1,0:T(8,128)S(1)} %get-tuple-element.37) | copy-start | bytes 786436
  98.9 13.8 %copy-start.7 = (f32[256,256]{1,0:T(8,128)}, f32[256,256]{1,0:T(8,128)S(1)}, u32[]{:S(2)}) copy-start(f32[256,256]{1,0:T(8,128)S(1)} %get-tuple-element.36) | copy-start | bytes 786436
  109.5 104.9 %all-gather.5.cloned.1.call-start = ((), (), s32[]{:S(2)}) async-start(), calls=%async_computation.1 | async-start | bytes 3538944 | tf_op jit(solution)/shard_map/all_gather | solution.py:70
  214.4 2.8 %copy-start.1 = (bf16[3072,512]{1,0:T(8,128)(2,1)S(1)}, bf16[3072,512]{1,0:T(8,128)(2,1)}, u32[]{:S(2)}) copy-start(bf16[3072,512]{1,0:T(8,128)(2,1)} %all-gather.5.cloned.1.call-done) | copy-start | bytes 9437188
Sparse Core Ops, SparseCore 0:
  16.6 77.8 all-reduce.2
  109.6 43.5 all-gather.2
  156.0 58.3 all-gather.4
where the time goes:
time: 226 us; the launch traced here: 225 us
  waiting for transfers between devices  180 us (80%)
  between operations  15.9 us (7%)
  matrix products  13 us (6%)
  blocking collectives  6.17 us (3%)
  local copies, waits for them, and re-layouts  6.12 us (3%)
  other arithmetic  4.39 us (2%)
    psum x1, waiting for transfers between devices, body(): lax.psum((key_part, value_part), ('fs', 'rep'))  77.9 us
    all_gather x1, waiting for transfers between devices, body(): lax.all_gather(value_weight_new.astype(jnp.bfloat16), ('fs', 'rep'), axis...  61.2 us
    all_gather x1, waiting for transfers between devices, body(): lax.all_gather(key_weight_new.astype(jnp.bfloat16), ('fs', 'rep'), axis=0...  40.5 us
    psum x1, blocking collectives, body(): squares = lax.psum(local_squares, 'tp')  6.17 us
    unnamed x28, local copies, waits for them, and re-layouts  6.12 us
  transfers between devices with their start and end apart: 3, of which 3 were waited for; matrix products, arithmetic and copies ran while one was open for 1% of the time, Pallas kernels for 0%

commit v1 on v0

--- a/solution.py
+++ b/solution.py
@@ -11,6 +11,18 @@
 second_decay = 0.9
 epsilon = 1e-08
 learn_rate = 0.01
+
+
+def collect(array, axis, dim):
+    ways, here = (lax.axis_size(axis), lax.axis_index(axis))
+    grown, reach = (array, 1)
+    while reach < ways:
+        theirs = lax.ppermute(grown, axis, [(d, d ^ reach) for d in range(ways)])
+        mine_first = jnp.concatenate([grown, theirs], axis=dim)
+        theirs_first = jnp.concatenate([theirs, grown], axis=dim)
+        grown = jnp.where(here & reach == 0, mine_first, theirs_first)
+        reach = 2 * reach
+    return grown
 
 
 def split_contract(basis, cotangent):
@@ -67,7 +79,7 @@
     value_weight_new = value_weight - learn_rate * value_step
     key_copy, value_copy = (
         lax.all_gather(key_weight_new.astype(jnp.bfloat16), ("fs", "rep"), axis=0, tiled=True),
-        lax.all_gather(value_weight_new.astype(jnp.bfloat16), ("fs", "rep"), axis=0, tiled=True),
+        collect(value_weight_new.astype(jnp.bfloat16), ("fs", "rep"), 0),
     )
     return (
         key_weight_new,

time: 226 us -> 238 us (1.053)
  waiting for transfers between devices: 180 us -> 187 us
  other arithmetic: 4.39 us -> 10.4 us
  local copies, waits for them, and re-layouts: 6.12 us -> 2.8 us
    ppermute x0 -> x3, waiting for transfers between devices: none -> 68.2 us  [collect(): theirs = lax.ppermute(grown, axis, [(d, d ^ reach) for d in range(ways)])]
    all_gather x1 -> x0, waiting for transfers between devices: 61.2 us -> none  [body(): lax.all_gather(value_weight_new.astype(jnp.bfloat16), ('fs', 'rep'), axis...]
    select_n x0 -> x3, other arithmetic: none -> 6.01 us  [collect(): grown = jnp.where(here & reach == 0, mine_first, theirs_first)]
    unnamed x28 -> x27, local copies, waits for them, and re-layouts: 6.12 us -> 2.8 us
  transfers between devices with their start and end apart: 3 -> 5, of which waited for: 3 -> 5; matrix products, arithmetic and copies ran while one was open for 1% -> 2% of each run, Pallas kernels for 0% -> 0%
where the time goes in v1:
time: 238 us
  waiting for transfers between devices  187 us (79%)
  between operations  16.2 us (7%)
  matrix products  13.1 us (6%)
  other arithmetic  10.4 us (4%)
  blocking collectives  6.17 us (3%)
  local copies, waits for them, and re-layouts  2.8 us (1%)
    psum x1, waiting for transfers between devices, body(): lax.psum((key_part, value_part), ('fs', 'rep'))  77.9 us
    ppermute x3, waiting for transfers between devices, collect(): theirs = lax.ppermute(grown, axis, [(d, d ^ reach) for d in range(ways)])  68.2 us
    all_gather x1, waiting for transfers between devices, body(): lax.all_gather(key_weight_new.astype(jnp.bfloat16), ('fs', 'rep'), axis=0...  40.9 us
    psum x1, blocking collectives, body(): squares = lax.psum(local_squares, 'tp')  6.17 us
    select_n x3, other arithmetic, collect(): grown = jnp.where(here & reach == 0, mine_first, theirs_first)  6.01 us
  transfers between devices with their start and end apart: 5, of which 5 were waited for; matrix products, arithmetic and copies ran while one was open for 2% of the time, Pallas kernels for 0%

profile of v1, /device:TPU:0, one launch (start us, length us, event | category | flops | bytes accessed | tf_op | source)
XLA Modules:
  0.0 237.7 jit_solution(7876751817787351936)
XLA Ops:
  7.2 0.0 copy-start
  7.2 0.0 copy-start.2
  7.2 0.0 all-reduce.3.cloned.1.call-start
  7.2 1.3 copy-done
  8.6 0.0 copy-start.12
  8.6 3.4 %fusion.17 = f32[640,256]{1,0:T(8,128)S(1)} fusion(bf16[640,3072]{1,0:T(8,128)(2,1)} %param.11, bf16[3072,256]{1,0:T(8,128)(2,1)S(1)} %copy-done), kind=kOutput, calls=%fused_computation.34 | convolution fusion | flops 1006632960 | bytes 6160384 | tf_op jit(solution)/shard_map/dot_general | solution.py:65
  12.0 0.0 copy-done.2
  12.1 0.4 fusion.5
  12.5 0.0 copy-start.11
  12.5 1.2 convolution_add_fusion
  13.7 0.0 copy-done.12
  13.7 0.3 copy-done.11
  13.9 0.0 copy-start.6
  13.9 1.2 fusion.16
  15.1 0.0 copy-done.6
  15.1 0.0 copy-start.9
  15.2 0.3 fusion.8
  15.5 1.0 convolution_add_fusion.1
  16.5 0.0 all-reduce.3.cloned.1.call-update
  16.5 0.0 all-gather.2.cloned.1.call-start
  16.6 77.9 %all-reduce.3.cloned.1.call-done = (f32[256,256]{1,0:T(8,128)}, f32[256,512]{1,0:T(8,128)}) async-done(((f32[256,256]{1,0:T(8,128)}, f32[256,512]{1,0:T(8,128)}), (f32[256,256]{1,0:T(8,128)}, f32[256,512]{1,0:T(8,128)})) %all-reduce.3.cloned.1.call-update) | async-done | bytes 786448 | tf_op jit(solution)/shard_map/psum | solution.py:67
  94.5 0.0 copy-start.10
  94.5 0.0 copy-done.9
  94.5 2.2 multiply_reduce_fusion
  96.7 0.0 copy-done.10
  96.7 2.2 multiply_reduce_fusion.1
  100.2 6.2 %psum.23 = f32[]{:T(128)} all-reduce(f32[]{:T(128)S(6)} %add.60), channel_id=1, replica_groups=mesh['fs'=4,'rep'=2,'tp'=4] {'tp'}, use_global_device_ids=true, to_apply=%region_4.0 | all-reduce | flops 1 | bytes 8 | tf_op jit(solution)/shard_map/psum | solution.py:73
  107.1 3.0 %fusion.12 = (bf16[384,512]{1,0:T(8,128)(2,1)S(1)}, f32[384,512]{1,0:T(8,128)}, f32[384,512]{1,0:T(8,128)}) fusion(f32[384,512]{1,0:T(8,128)} %param.17, f32[256,512]{1,0:T(8,128)S(1)} %get-tuple-element.38, f32[256,512]{1,0:T(8,128)S(1)} %get-tuple-element.39, bf16[3072,256]{1,0:T(8,128)(2,1)S(1)} %copy-done, s32[]{:T(128)S(6)} %select_n.28, f32[]{:T(128)S(6)} %sqrt.11), kind=kOutput, calls=%fused_computation.31 | convolution fusion | flops 605028352 | bytes 3997704 | tf_op jit(solution)/shard_map/dot_general | solution.py:77
  110.1 0.0 copy-done.3
  110.1 0.0 copy-done.4
  110.1 0.8 collective-permute-start
  110.9 0.0 copy-done.7
  110.9 0.0 copy-done.8
  110.9 2.5 %fusion.13 = (bf16[384,256]{1,0:T(8,128)(2,1)}, f32[384,256]{1,0:T(8,128)}, f32[384,256]{1,0:T(8,128)}) fusion(f32[384,256]{1,0:T(8,128)} %param.16, f32[256,256]{1,0:T(8,128)S(1)} %get-tuple-element.36, f32[256,256]{1,0:T(8,128)S(1)} %get-tuple-element.37, bf16[3072,256]{1,0:T(8,128)(2,1)} %param.14, s32[]{:T(128)S(6)} %select_n.28, f32[]{:T(128)S(6)} %sqrt.11), kind=kOutput, calls=%fused_computation.32 | convolution fusion | flops 302514176 | bytes 2097160 | tf_op jit(solution)/shard_map/dot_general | solution.py:76
  113.4 0.0 all-gather.2.cloned.1.call-update
  113.4 7.6 %collective-permute-done = bf16[384,512]{1,0:T(8,128)(2,1)S(1)} collective-permute-done((bf16[384,512]{1,0:T(8,128)(2,1)S(1)}, bf16[384,512]{1,0:T(8,128)(2,1)S(1)}, u32[]{:S(2)}, u32[]{:S(2)}) %collective-permute-start) | collective-permute-done | bytes 393248 | tf_op jit(solution)/shard_map/ppermute | solution.py:20
  121.0 0.3 maximum_select_fusion.2
  121.3 0.0 copy-start.1
  121.3 1.0 collective-permute-start.1
  122.4 0.0 copy-done.1
  122.4 30.3 %collective-permute-done.1 = bf16[768,512]{1,0:T(8,128)(2,1)} collective-permute-done((bf16[768,512]{1,0:T(8,128)(2,1)S(1)}, bf16[768,512]{1,0:T(8,128)(2,1)}, u32[]{:S(2)}, u32[]{:S(2)}) %collective-permute-start.1) | collective-permute-done | bytes 786464 | tf_op jit(solution)/shard_map/ppermute | solution.py:20
  152.7 2.3 maximum_select_fusion.1
  155.0 0.1 collective-permute-start.2
  155.1 40.9 %all-gather.2.cloned.1.call-done = bf16[3072,256]{1,0:T(8,128)(2,1)} async-done(((bf16[384,256]{1,0:T(8,128)(2,1)}), bf16[3072,256]{1,0:T(8,128)(2,1)}) %all-gather.2.cloned.1.call-update) | async-done | bytes 1572880 | tf_op jit(solution)/shard_map/all_gather | solution.py:81
  196.0 30.3 %collective-permute-done.2 = bf16[1536,512]{1,0:T(8,128)(2,1)} collective-permute-done((bf16[1536,512]{1,0:T(8,128)(2,1)S(1)}, bf16[1536,512]{1,0:T(8,128)(2,1)}, u32[]{:S(2)}, u32[]{:S(2)}) %collective-permute-start.2) | collective-permute-done | bytes 1572896 | tf_op jit(solution)/shard_map/ppermute | solution.py:20
  226.3 3.4 %maximum_select_fusion = bf16[3072,512]{1,0:T(8,128)(2,1)} fusion(bf16[1536,512]{1,0:T(8,128)(2,1)} %collective-permute-done.2, bf16[1536,512]{1,0:T(8,128)(2,1)S(1)} %maximum_select_fusion.1, pred[]{:T(512)S(6)} %eq.9), kind=kLoop, calls=%fused_computation | loop fusion | flops 14155776 | bytes 6291457 | tf_op jit(solution)/shard_map/jit(_where)/select_n | solution.py:23
  229.7 0.0 copy-done.5
  229.7 1.1 copy.24
  (5 shorter events, 0.0 us)
Async XLA Ops:
  7.2 1.4 copy-start
  7.2 4.9 %copy-start.2 = (bf16[640,512]{1,0:T(8,128)(2,1)S(1)}, bf16[640,512]{1,0:T(8,128)(2,1)}, u32[]{:S(2)}) copy-start(bf16[640,512]{1,0:T(8,128)(2,1)} %param.13) | copy-start | bytes 1966084
  7.2 87.3 %all-reduce.3.cloned.1.call-start = ((), (), s32[]{:S(2)}) async-start(), calls=%async_computation.1 | async-start | bytes 1572864 | tf_op jit(solution)/shard_map/psum | solution.py:67
  8.6 5.1 %copy-start.12 = (bf16[640,3072]{1,0:T(8,128)(2,1)S(1)}, bf16[640,3072]{1,0:T(8,128)(2,1)}, u32[]{:S(2)}) copy-start(bf16[640,3072]{1,0:T(8,128)(2,1)} %param.11) | copy-start | bytes 11796484
  12.5 1.5 copy-start.11
  13.9 1.2 copy-start.6
  15.1 79.4 %copy-start.9 = (f32[256,512]{1,0:T(8,128)S(1)}, f32[256,512]{1,0:T(8,128)}, u32[]{:S(2)}) copy-start(f32[256,512]{1,0:T(8,128)} %param.21) | copy-start | bytes 1572868
  16.5 179.5 %all-gather.2.cloned.1.call-start = ((), (), s32[]{:S(2)}) async-start(), calls=%async_computation | async-start | bytes 1769472 | tf_op jit(solution)/shard_map/all_gather | solution.py:81
  94.5 2.2 copy-start.10
  96.7 13.4 %copy-start.3 = (f32[256,512]{1,0:T(8,128)}, f32[256,512]{1,0:T(8,128)S(1)}, u32[]{:S(2)}) copy-start(f32[256,512]{1,0:T(8,128)S(1)} %get-tuple-element.39) | copy-start | bytes 1572868
  96.7 13.4 %copy-start.4 = (f32[256,512]{1,0:T(8,128)}, f32[256,512]{1,0:T(8,128)S(1)}, u32[]{:S(2)}) copy-start(f32[256,512]{1,0:T(8,128)S(1)} %get-tuple-element.38) | copy-start | bytes 1572868
  98.9 12.1 %copy-start.7 = (f32[256,256]{1,0:T(8,128)}, f32[256,256]{1,0:T(8,128)S(1)}, u32[]{:S(2)}) copy-start(f32[256,256]{1,0:T(8,128)S(1)} %get-tuple-element.37) | copy-start | bytes 786436
  98.9 12.1 %copy-start.8 = (f32[256,256]{1,0:T(8,128)}, f32[256,256]{1,0:T(8,128)S(1)}, u32[]{:S(2)}) copy-start(f32[256,256]{1,0:T(8,128)S(1)} %get-tuple-element.36) | copy-start | bytes 786436
  110.1 10.9 %collective-permute-start = (bf16[384,512]{1,0:T(8,128)(2,1)S(1)}, bf16[384,512]{1,0:T(8,128)(2,1)S(1)}, u32[]{:S(2)}, u32[]{:S(2)}) collective-permute-start(bf16[384,512]{1,0:T(8,128)(2,1)S(1)} %get-tuple-element.12), channel_id=1, source_target_pairs={{0,4},{4,0},{8,12},{12,8},{16,20},{20,16},{24,28},{28,24},{1,5},{5... | collective-permute-start | bytes 1179656 | tf_op jit(solution)/shard_map/ppermute | solution.py:20
  121.3 1.1 copy-start.1
  121.3 31.4 %collective-permute-start.1 = (bf16[768,512]{1,0:T(8,128)(2,1)S(1)}, bf16[768,512]{1,0:T(8,128)(2,1)}, u32[]{:S(2)}, u32[]{:S(2)}) collective-permute-start(bf16[768,512]{1,0:T(8,128)(2,1)S(1)} %maximum_select_fusion.2), channel_id=1, source_target_pairs={{0,8},{4,12},{8,0},{12,4},{16,24},{20,28},{24,16},{28,20},{1,9},{5... | collective-permute-start | bytes 2359304 | tf_op jit(solution)/shard_map/ppermute | solution.py:20
  155.0 71.3 %collective-permute-start.2 = (bf16[1536,512]{1,0:T(8,128)(2,1)S(1)}, bf16[1536,512]{1,0:T(8,128)(2,1)}, u32[]{:S(2)}, u32[]{:S(2)}) collective-permute-start(bf16[1536,512]{1,0:T(8,128)(2,1)S(1)} %maximum_select_fusion.1), channel_id=1, source_target_pairs={{0,16},{4,20},{8,24},{12,28},{16,0},{20,4},{24,8},{28,12},{1,17},{... | collective-permute-start | bytes 4718600 | tf_op jit(solution)/shard_map/ppermute | solution.py:20
  196.0 33.7 %copy-start.5 = (bf16[3072,256]{1,0:T(8,128)(2,1)S(1)}, bf16[3072,256]{1,0:T(8,128)(2,1)}, u32[]{:S(2)}) copy-start(bf16[3072,256]{1,0:T(8,128)(2,1)} %all-gather.2.cloned.1.call-done) | copy-start | bytes 4718596
Sparse Core Ops, SparseCore 0:
  16.6 77.8 all-reduce.2
  113.6 82.3 all-gather.1
